TPU v7x, 32 devices: a whole 2x2x4 slice. The times are simulated.
32 devices in a mesh: grp: 2 (over y), ep: 8 (over z, x), tp: 2 (over core).
Axes of the slice: x: 2, y: 2, z: 4, core: 2. Of those that a mesh axis runs over, the one named last changes fastest.
Arguments:
- tokens: bfloat16 [2048, 2048], P(('grp', 'ep')), parts along dimension 0, may hold values from -6 to 6
- in_gain: float32 [2048], replicated, may hold values from 0.1 to 1.9
- routing: int32 [2048, 4], P(('grp', 'ep')), parts along dimension 0, may hold values from 0 to 15, as said below
- gate_prob: float32 [2048, 4], P(('grp', 'ep')), parts along dimension 0, may hold values from 0.05 to 1
- w_gate: bfloat16 [16, 2048, 512], P('ep', None, 'tp'), may hold values from -0.125 to 0.125
- w_up: bfloat16 [16, 2048, 512], P('ep', None, 'tp'), may hold values from -0.125 to 0.125
- w_down: bfloat16 [16, 512, 2048], P('ep', 'tp')
- out_gain: float32 [2048], P('tp'), may hold values from 0.1 to 1.9
Outputs:
- output: bfloat16 [2048, 2048], P(('grp', 'ep'), 'tp'), parts along dimension 0
There are 2 independent parts, one for each index of `grp`. A program takes and returns all parts, laid end to end along the dimension named above; an argument that names none is the same for every part. Nothing has to cross between parts.
Inputs may be any that keep to these rules, and one draw needn't show every extreme that they name: `routing`: each row names 4 different experts, all of one group (the same value of expert // 4). In the rows of one device no expert is named more than 64 times, and in every device's rows some expert is named exactly 64 times.
All inputs are finite; a program needn't handle non-finite values.
Results may differ from a plain program's by a relative error of at most 0.0077.
Values may be sent and summed in bfloat16 or wider, within the bound.
A program may use at most 64 MiB of HBM per device.

v0:
```python
import jax
import jax.numpy as jnp
from jax import lax
from jax.sharding import PartitionSpec as P

GROUPS = 4
EPS = 1e-06


def slot_ranks(flat_routes, expert_count):
    matches = (flat_routes[:, None] == jnp.arange(expert_count, dtype=jnp.int32)[None, :]).astype(
        jnp.int32
    )
    earlier = jnp.cumsum(matches, axis=0) - matches
    return jnp.sum(earlier * matches, axis=1)


def fill_rows(source, entries):
    filled = entries > 0
    return jnp.where(
        filled[:, None], source[jnp.maximum(entries - 1, 0)], jnp.zeros((), source.dtype)
    )


def body(tokens, in_gain, routing, gate_prob, w_gate, w_up, w_down, out_gain):
    ep_count = lax.axis_size("ep")
    local_experts = w_gate.shape[0]
    expert_count = local_experts * ep_count
    tok_dev, top_count = routing.shape
    model_width = tokens.shape[1]
    half_width = out_gain.shape[0]
    group_width = expert_count // GROUPS
    row_cap = max(2, tok_dev * top_count // (2 * group_width))
    floats = tokens.astype(jnp.float32)
    normed = (
        floats * lax.rsqrt(jnp.mean(floats * floats, axis=-1, keepdims=True) + EPS) * in_gain
    ).astype(jnp.bfloat16)
    flat_routes = routing.reshape(-1)
    slot_rank = slot_ranks(flat_routes, expert_count)
    slot_ids = flat_routes * row_cap + slot_rank
    token_ids = jnp.arange(tok_dev * top_count, dtype=jnp.int32) // top_count
    slot_table = jnp.zeros((expert_count * row_cap,), jnp.int32).at[slot_ids].set(token_ids + 1)
    own_columns = lax.dynamic_slice_in_dim(normed, lax.axis_index("tp") * half_width, half_width, 1)
    sendbuf = fill_rows(own_columns, slot_table).reshape(
        ep_count, local_experts, row_cap, half_width
    )
    arrived = lax.all_to_all(sendbuf, "ep", split_axis=0, concat_axis=0, tiled=True)
    arrived = lax.all_gather(arrived, "tp", axis=3, tiled=True)
    gate_act = jnp.einsum("secd,edf->secf", arrived, w_gate, preferred_element_type=jnp.float32)
    up_act = jnp.einsum("secd,edf->secf", arrived, w_up, preferred_element_type=jnp.float32)
    hidden = (jax.nn.silu(gate_act) * up_act).astype(jnp.bfloat16)
    partial_out = jnp.einsum("secf,efd->secd", hidden, w_down, preferred_element_type=jnp.float32)
    results = lax.psum_scatter(
        partial_out.astype(jnp.bfloat16), "tp", scatter_dimension=3, tiled=True
    )
    returned = lax.all_to_all(results, "ep", split_axis=0, concat_axis=0, tiled=True).reshape(
        expert_count * row_cap, half_width
    )
    picked = returned[slot_ids].astype(jnp.float32).reshape(tok_dev, top_count, half_width)
    mixed_rows = jnp.sum(picked * gate_prob[:, :, None], axis=1)
    squares = jnp.sum(mixed_rows * mixed_rows, axis=1)
    total_squares = lax.psum(squares, "tp")
    inv_rms = lax.rsqrt(total_squares / model_width + EPS)
    return (mixed_rows * inv_rms[:, None] * out_gain).astype(jnp.bfloat16)


def solution(mesh):
    placed = (
        P(("grp", "ep"), None),
        P(),
        P(("grp", "ep"), None),
        P(("grp", "ep"), None),
        P("ep", None, "tp"),
        P("ep", None, "tp"),
        P("ep", "tp", None),
        P("tp"),
    )
    return jax.shard_map(
        body, mesh=mesh, in_specs=placed, out_specs=P(("grp", "ep"), "tp"), check_vma=False
    )
```

profile of v0, /device:TPU:0, one launch (start us, length us, event | category | flops | bytes accessed | tf_op | source)
XLA Modules:
  0.0 192.8 jit_solution(13421549271625434358)
XLA Ops:
  6.5 0.0 copy-start
  6.5 0.0 copy-start.1
  6.5 0.0 copy-start.4
  6.5 0.0 all-gather.2.cloned.1.call-start
  6.6 1.3 convert_element_type.34
  7.8 1.2 multiply_reduce_fusion.1
  9.1 0.0 copy-done.1
  9.1 0.1 copy.19
  9.2 0.1 eq.29
  9.3 0.1 eq.25
  9.4 1.2 reduce-window.6
  10.6 0.2 slice_reduce_fusion
  10.9 0.1 copy.18
  11.0 0.1 mul.77
  11.1 0.1 fusion.24
  11.2 2.4 %scatter_custom_fusion = s32[1024]{0:T(1024)S(1)} fusion(s32[512]{0:T(512)S(1)} %bitcast.63, s32[512]{0:T(512)S(1)} %fusion.26, s32[]{:T(128)} %constant.19.clone.1), kind=kCustom, calls=%fused_computation.42 | custom fusion | bytes 4100 | tf_op jit(solution)/shard_map/scatter | solution.py:42
  13.7 0.1 broadcast_in_dim.16
  13.8 0.0 copy-done.4
  13.8 0.1 fusion.20
  13.9 5.4 %gather_fusion = bf16[1024,1024]{1,0:T(8,128)(2,1)} fusion(bf16[128,1024]{1,0:T(8,128)(2,1)S(1)} %fusion.20, s32[1024]{0:T(1024)S(1)} %maximum_clamp_fusion), kind=kCustom, calls=%fused_computation | custom fusion | bytes 4198400 | tf_op jit(solution)/shard_map/gather | solution.py:21
  19.3 1.8 broadcast_select_fusion
  21.1 55.3 %all_to_all.10 = bf16[8,2,64,1024]{3,2,1,0:T(8,128)(2,1)S(1)} all-to-all(bf16[8,2,64,1024]{3,2,1,0:T(8,128)(2,1)S(1)} %broadcast_select_fusion), channel_id=1, replica_groups=mesh['grp'=2,'ep'=8,'tp'=2] {'ep'}, dimensions={0} | all-to-all | bytes 4194304 | tf_op jit(solution)/shard_map/all_to_all | solution.py:47
  76.4 1.5 copy.22
  77.9 0.0 all-gather.2.cloned.1.call-update
  78.0 0.0 reduce-scatter.2.cloned.1.call-start
  78.0 12.8 %all-gather.2.cloned.1.call-done = bf16[8,2,64,2048]{3,2,0,1:T(8,128)(2,1)} async-done(((bf16[8,2,64,1024]{3,2,0,1:T(8,128)(2,1)}), bf16[8,2,64,2048]{3,2,0,1:T(8,128)(2,1)}) %all-gather.2.cloned.1.call-update) | async-done | bytes 4194320 | tf_op jit(solution)/shard_map/all_gather | solution.py:48
  90.8 4.1 %fusion.5 = f32[8,2,64,256]{3,2,0,1:T(8,128)S(1)} fusion(bf16[8,2,64,2048]{3,2,0,1:T(8,128)(2,1)} %all-gather.2.cloned.1.call-done, bf16[2,2048,256]{2,1,0:T(8,128)(2,1)} %param.12), kind=kOutput, calls=%fused_computation.11 | convolution fusion | flops 1073741824 | bytes 7340032 | tf_op jit(solution)/shard_map/secd,edf->secf/dot_general | solution.py:49
  94.9 0.0 copy-done
  94.9 7.3 %convert_bitcast_fusion = bf16[8,2,64,2048]{3,2,0,1:T(8,128)(2,1)} fusion(bf16[2,256,2048]{2,1,0:T(8,128)(2,1)S(1)} %copy-done, bf16[8,2,64,2048]{3,2,0,1:T(8,128)(2,1)} %all-gather.2.cloned.1.call-done, bf16[2,2048,256]{2,1,0:T(8,128)(2,1)} %param.13, f32[8,2,64,256]{3,2,0,1:T(8,128)S(1)} %fusion.5), kind=kOutput, calls=%fused_computation.3 | convolution fusion | flops 2151153664 | bytes 13631488 | tf_op jit(solution)/shard_map/secf,efd->secd/dot_general | solution.py:52
  102.2 0.0 reduce-scatter.2.cloned.1.call-update
  102.3 13.2 %reduce-scatter.2.cloned.1.call-done = bf16[8,2,64,1024]{3,2,0,1:T(8,128)(2,1)} async-done(((bf16[8,2,64,2048]{3,2,0,1:T(8,128)(2,1)}), bf16[8,2,64,1024]{3,2,0,1:T(8,128)(2,1)}) %reduce-scatter.2.cloned.1.call-update) | async-done | bytes 2097168 | tf_op jit(solution)/shard_map/reduce_scatter | solution.py:53
  115.5 3.1 %copy.23 = bf16[8,2,64,1024]{3,2,1,0:T(8,128)(2,1)} copy(bf16[8,2,64,1024]{3,2,0,1:T(8,128)(2,1)} %reduce-scatter.2.cloned.1.call-done) | data formatting | bytes 4194304 | tf_op jit(solution)/shard_map/reduce_scatter | solution.py:53
  118.6 0.0 copy-start.3
  118.6 6.0 %all-to-all-start.1 = ((bf16[8,2,64,1024]{3,2,1,0:T(8,128)(2,1)}), bf16[8,2,64,1024]{3,2,1,0:T(8,128)(2,1)}, u32[]{:S(2)}, u32[]{:S(2)}) async-start(bf16[8,2,64,1024]{3,2,1,0:T(8,128)(2,1)} %copy.23), calls=%async_computation.2 | async-start | bytes 4194304 | tf_op jit(solution)/shard_map/all_to_all | solution.py:56
  124.6 0.0 copy-done.3
  124.6 0.1 copy.24
  124.7 48.5 %all-to-all-done.1 = bf16[8,2,64,1024]{3,2,1,0:T(8,128)(2,1)} async-done(((bf16[8,2,64,1024]{3,2,1,0:T(8,128)(2,1)}), bf16[8,2,64,1024]{3,2,1,0:T(8,128)(2,1)}, u32[]{:S(2)}, u32[]{:S(2)}) %all-to-all-start.1) | async-done | bytes 2097184 | tf_op jit(solution)/shard_map/all_to_all | solution.py:56
  173.3 4.6 %gather_fusion.1 = bf16[512,1024]{1,0:T(8,128)(2,1)S(1)} fusion(bf16[1024,1024]{1,0:T(8,128)(2,1)} %bitcast.13, s32[1024]{0:T(1024)S(1)} %pad_clamp_fusion), kind=kCustom, calls=%fused_computation.1 | custom fusion | bytes 2099200 | tf_op jit(solution)/shard_map/gather | solution.py:59
  177.9 1.7 reshape.75
  179.6 0.0 copy-start.2
  179.6 3.0 %multiply_reduce_fusion = f32[128,1024]{1,0:T(8,128)S(1)} fusion(f32[128,4,1024]{2,1,0:T(4,128)} %reshape.75, f32[128,4]{1,0:T(8,128)S(1)} %copy.24), kind=kLoop, calls=%fused_computation.9 | loop fusion | flops 917504 | bytes 2623488 | tf_op jit(solution)/shard_map/reduce_sum | solution.py:60
  182.6 0.1 multiply_reduce_fusion.2
  182.7 2.5 %psum.7 = f32[128]{0:T(128)S(1)} all-reduce(f32[128]{0:T(128)S(1)} %multiply_reduce_fusion.2), channel_id=1, replica_groups=mesh['grp'=2,'ep'=8,'tp'=2] {'tp'}, use_global_device_ids=true, to_apply=%region_8.9 | all-reduce | flops 128 | bytes 1024 | tf_op jit(solution)/shard_map/psum | solution.py:62
  185.2 0.0 copy-done.2
  185.2 0.8 multiply_convert_fusion
  (12 shorter events, 0.1 us)
Async XLA Ops:
  6.5 88.4 %copy-start = (bf16[2,256,2048]{2,1,0:T(8,128)(2,1)S(1)}, bf16[2,256,2048]{2,1,0:T(8,128)(2,1)}, u32[]{:S(2)}) copy-start(bf16[2,256,2048]{2,1,0:T(8,128)(2,1)} %param.14) | copy-start | bytes 6291460
  6.5 2.5 %copy-start.1 = (s32[128,4]{0,1:T(4,128)S(1)}, s32[128,4]{0,1:T(4,128)}, u32[]{:S(2)}) copy-start(s32[128,4]{0,1:T(4,128)} %param.10) | copy-start | bytes 6148
  6.5 7.2 %copy-start.4 = (f32[2048]{0:T(1024)S(1)}, f32[2048]{0:T(1024)}, u32[]{:S(2)}) copy-start(f32[2048]{0:T(1024)} %param.9) | copy-start | bytes 24580
  6.5 84.3 %all-gather.2.cloned.1.call-start = ((), (), s32[]{:S(2)}) async-start(), calls=%async_computation.3 | async-start | bytes 6291456 | tf_op jit(solution)/shard_map/all_gather | solution.py:48
  78.0 37.5 %reduce-scatter.2.cloned.1.call-start = ((), (), s32[]{:S(2)}) async-start(), calls=%async_computation.4 | async-start | bytes 6291456 | tf_op jit(solution)/shard_map/reduce_scatter | solution.py:53
  118.6 6.0 %copy-start.3 = (f32[128,4]{0,1:T(4,128)S(1)}, f32[128,4]{0,1:T(4,128)}, u32[]{:S(2)}) copy-start(f32[128,4]{0,1:T(4,128)} %param.11) | copy-start | bytes 6148
  118.6 54.7 %all-to-all-start.1 = ((bf16[8,2,64,1024]{3,2,1,0:T(8,128)(2,1)}), bf16[8,2,64,1024]{3,2,1,0:T(8,128)(2,1)}, u32[]{:S(2)}, u32[]{:S(2)}) async-start(bf16[8,2,64,1024]{3,2,1,0:T(8,128)(2,1)} %copy.23), calls=%async_computation.2 | async-start | bytes 4194304 | tf_op jit(solution)/shard_map/all_to_all | solution.py:56
  179.6 5.6 %copy-start.2 = (f32[1024]{0:T(1024)S(1)}, f32[1024]{0:T(1024)}, u32[]{:S(2)}) copy-start(f32[1024]{0:T(1024)} %param.15) | copy-start | bytes 12292
Sparse Core Ops, SparseCore 0:
  78.1 12.6 all-gather.1
  102.4 13.0 reduce-scatter.1
where the time goes:
time: 193 us
  waiting for transfers between devices  74.6 us (39%)
  blocking collectives  57.8 us (30%)
  local copies, waits for them, and re-layouts  19.8 us (10%)
  between operations  13.6 us (7%)
  matrix products  11.4 us (6%)
  other arithmetic  9.68 us (5%)
  starting transfers between devices  6.06 us (3%)
    all_to_all x1, blocking collectives, body(): lax.all_to_all(sendbuf, 'ep', split_axis=0, concat_axis=0, tiled=True)  55.3 us
    all_to_all x1, waiting for transfers between devices, body(): lax.all_to_all(results, 'ep', split_axis=0, concat_axis=0, tiled=True)  48.5 us
    reduce_scatter x1, waiting for transfers between devices, body(): lax.psum_scatter(partial_out.astype(jnp.bfloat16), 'tp', scatter_dimensio...  13.2 us
    all_gather x1, waiting for transfers between devices, body(): arrived = lax.all_gather(arrived, 'tp', axis=3, tiled=True)  12.8 us
    dot_general x1, matrix products, body(): jnp.einsum('secf,efd->secd', hidden, w_down, preferred_element_type=jnp.f...  7.3 us
    all_to_all x1, starting transfers between devices, body(): lax.all_to_all(results, 'ep', split_axis=0, concat_axis=0, tiled=True)  6.02 us
    gather x1, local copies, waits for them, and re-layouts, fill_rows(): source[jnp.maximum(entries - 1, 0)]  5.36 us
    gather x1, local copies, waits for them, and re-layouts, body(): returned[slot_ids].astype(jnp.float32)  4.59 us
  transfers between devices with their start and end apart: 3, of which 3 were waited for; matrix products, arithmetic and copies ran while one was open for 0% of the time, Pallas kernels for 0%

commit v1 on v0

--- a/solution.py
+++ b/solution.py
@@ -45,7 +45,7 @@
         ep_count, local_experts, row_cap, half_width
     )
     arrived = lax.all_to_all(sendbuf, "ep", split_axis=0, concat_axis=0, tiled=True)
-    arrived = lax.all_gather(arrived, "tp", axis=3, tiled=True)
+    arrived = jnp.concatenate(lax.all_gather(arrived, "tp"), axis=3)
     gate_act = jnp.einsum("secd,edf->secf", arrived, w_gate, preferred_element_type=jnp.float32)
     up_act = jnp.einsum("secd,edf->secf", arrived, w_up, preferred_element_type=jnp.float32)
     hidden = (jax.nn.silu(gate_act) * up_act).astype(jnp.bfloat16)

time: 193 us -> 208 us (1.078)
  local copies, waits for them, and re-layouts: 19.8 us -> 34.5 us
    reshape x0 -> x2, local copies, waits for them, and re-layouts: none -> 16.3 us  [body(): arrived = jnp.concatenate(lax.all_gather(arrived, 'tp'), axis=3)]
where the time goes in v1:
time: 208 us
  waiting for transfers between devices  74.6 us (36%)
  blocking collectives  57.9 us (28%)
  local copies, waits for them, and re-layouts  34.5 us (17%)
  between operations  13.6 us (7%)
  matrix products  11.4 us (5%)
  other arithmetic  9.68 us (5%)
  starting transfers between devices  6.07 us (3%)
    all_to_all x1, blocking collectives, body(): lax.all_to_all(sendbuf, 'ep', split_axis=0, concat_axis=0, tiled=True)  55.4 us
    all_to_all x1, waiting for transfers between devices, body(): lax.all_to_all(results, 'ep', split_axis=0, concat_axis=0, tiled=True)  48.5 us
    reshape x2, local copies, waits for them, and re-layouts, body(): arrived = jnp.concatenate(lax.all_gather(arrived, 'tp'), axis=3)  16.3 us
    reduce_scatter x1, waiting for transfers between devices, body(): lax.psum_scatter(partial_out.astype(jnp.bfloat16), 'tp', scatter_dimensio...  13.2 us
    all_gather x1, waiting for transfers between devices, body(): arrived = jnp.concatenate(lax.all_gather(arrived, 'tp'), axis=3)  12.8 us
    dot_general x1, matrix products, body(): jnp.einsum('secf,efd->secd', hidden, w_down, preferred_element_type=jnp.f...  7.3 us
    all_to_all x1, starting transfers between devices, body(): lax.all_to_all(results, 'ep', split_axis=0, concat_axis=0, tiled=True)  6.02 us
    gather x1, local copies, waits for them, and re-layouts, fill_rows(): source[jnp.maximum(entries - 1, 0)]  5.36 us
  transfers between devices with their start and end apart: 3, of which 3 were waited for; matrix products, arithmetic and copies ran while one was open for 0% of the time, Pallas kernels for 0%

profile of v1, /device:TPU:0, one launch (start us, length us, event | category | flops | bytes accessed | tf_op | source)
XLA Modules:
  0.0 207.7 jit_solution(15831142377028312146)
XLA Ops:
  6.5 0.0 copy-start
  6.5 0.0 copy-start.1
  6.5 0.0 copy-start.4
  6.5 0.0 all-gather.3.cloned.1.call-start
  6.6 1.3 convert_element_type.34
  7.8 1.2 multiply_reduce_fusion.1
  9.1 0.0 copy-done.1
  9.1 0.1 copy.18
  9.2 0.1 eq.29
  9.3 0.1 eq.25
  9.4 1.2 reduce-window.6
  10.6 0.2 slice_reduce_fusion
  10.9 0.1 copy.17
  11.0 0.1 mul.77
  11.1 0.1 fusion.24
  11.2 2.4 %scatter_custom_fusion = s32[1024]{0:T(1024)S(1)} fusion(s32[512]{0:T(512)S(1)} %bitcast.69, s32[512]{0:T(512)S(1)} %fusion.26, s32[]{:T(128)} %constant.19.clone.1), kind=kCustom, calls=%fused_computation.42 | custom fusion | bytes 4100 | tf_op jit(solution)/shard_map/scatter | solution.py:42
  13.7 0.1 broadcast_in_dim.16
  13.8 0.0 copy-done.4
  13.8 0.1 fusion.20
  13.9 5.4 %gather_fusion = bf16[1024,1024]{1,0:T(8,128)(2,1)} fusion(bf16[128,1024]{1,0:T(8,128)(2,1)S(1)} %fusion.20, s32[1024]{0:T(1024)S(1)} %maximum_clamp_fusion), kind=kCustom, calls=%fused_computation | custom fusion | bytes 4198400 | tf_op jit(solution)/shard_map/gather | solution.py:21
  19.3 1.8 broadcast_select_fusion
  21.1 55.4 %all_to_all.10 = bf16[8,2,64,1024]{3,2,1,0:T(8,128)(2,1)} all-to-all(bf16[8,2,64,1024]{3,2,1,0:T(8,128)(2,1)S(1)} %broadcast_select_fusion), channel_id=1, replica_groups=mesh['grp'=2,'ep'=8,'tp'=2] {'ep'}, dimensions={0} | all-to-all | bytes 4194304 | tf_op jit(solution)/shard_map/all_to_all | solution.py:47
  76.5 0.0 all-gather.3.cloned.1.call-update
  76.5 0.0 reduce-scatter.2.cloned.1.call-start
  76.6 12.8 %all-gather.3.cloned.1.call-done = bf16[16,2,64,1024]{3,2,1,0:T(8,128)(2,1)} async-done(((bf16[8,2,64,1024]{3,2,1,0:T(8,128)(2,1)}), bf16[16,2,64,1024]{3,2,1,0:T(8,128)(2,1)}) %all-gather.3.cloned.1.call-update) | async-done | bytes 4194320 | tf_op jit(solution)/shard_map/all_gather | solution.py:48
  89.4 8.5 %copy.21 = bf16[8,2,64,2,1024]{4,3,2,0,1:T(2,128)(2,1)} copy(bf16[8,2,64,2,1024]{4,2,1,0,3:T(8,128)(2,1)} %bitcast.68) | data formatting | bytes 8388608 | tf_op jit(solution)/shard_map/reshape | solution.py:48
  97.9 7.8 %reshape.81 = bf16[8,2,64,2048]{3,2,0,1:T(8,128)(2,1)} reshape(bf16[8,2,64,2,1024]{4,3,2,0,1:T(2,128)(2,1)} %copy.21) | data formatting | bytes 8388608 | tf_op jit(solution)/shard_map/reshape | solution.py:48
  105.6 4.1 %fusion.5 = f32[8,2,64,256]{3,2,0,1:T(8,128)S(1)} fusion(bf16[8,2,64,2048]{3,2,0,1:T(8,128)(2,1)} %reshape.81, bf16[2,2048,256]{2,1,0:T(8,128)(2,1)} %param.12), kind=kOutput, calls=%fused_computation.11 | convolution fusion | flops 1073741824 | bytes 7340032 | tf_op jit(solution)/shard_map/secd,edf->secf/dot_general | solution.py:49
  109.8 0.0 copy-done
  109.8 7.3 %convert_bitcast_fusion = bf16[8,2,64,2048]{3,2,0,1:T(8,128)(2,1)} fusion(bf16[2,256,2048]{2,1,0:T(8,128)(2,1)S(1)} %copy-done, bf16[8,2,64,2048]{3,2,0,1:T(8,128)(2,1)} %reshape.81, bf16[2,2048,256]{2,1,0:T(8,128)(2,1)} %param.13, f32[8,2,64,256]{3,2,0,1:T(8,128)S(1)} %fusion.5), kind=kOutput, calls=%fused_computation.3 | convolution fusion | flops 2151153664 | bytes 13631488 | tf_op jit(solution)/shard_map/secf,efd->secd/dot_general | solution.py:52
  117.1 0.0 reduce-scatter.2.cloned.1.call-update
  117.1 13.2 %reduce-scatter.2.cloned.1.call-done = bf16[8,2,64,1024]{3,2,0,1:T(8,128)(2,1)} async-done(((bf16[8,2,64,2048]{3,2,0,1:T(8,128)(2,1)}), bf16[8,2,64,1024]{3,2,0,1:T(8,128)(2,1)}) %reduce-scatter.2.cloned.1.call-update) | async-done | bytes 2097168 | tf_op jit(solution)/shard_map/reduce_scatter | solution.py:53
  130.3 3.1 %copy.22 = bf16[8,2,64,1024]{3,2,1,0:T(8,128)(2,1)} copy(bf16[8,2,64,1024]{3,2,0,1:T(8,128)(2,1)} %reduce-scatter.2.cloned.1.call-done) | data formatting | bytes 4194304 | tf_op jit(solution)/shard_map/reduce_scatter | solution.py:53
  133.4 0.0 copy-start.3
  133.4 6.0 %all-to-all-start.1 = ((bf16[8,2,64,1024]{3,2,1,0:T(8,128)(2,1)}), bf16[8,2,64,1024]{3,2,1,0:T(8,128)(2,1)}, u32[]{:S(2)}, u32[]{:S(2)}) async-start(bf16[8,2,64,1024]{3,2,1,0:T(8,128)(2,1)} %copy.22), calls=%async_computation.2 | async-start | bytes 4194304 | tf_op jit(solution)/shard_map/all_to_all | solution.py:56
  139.4 0.0 copy-done.3
  139.5 0.1 copy.23
  139.6 48.5 %all-to-all-done.1 = bf16[8,2,64,1024]{3,2,1,0:T(8,128)(2,1)} async-done(((bf16[8,2,64,1024]{3,2,1,0:T(8,128)(2,1)}), bf16[8,2,64,1024]{3,2,1,0:T(8,128)(2,1)}, u32[]{:S(2)}, u32[]{:S(2)}) %all-to-all-start.1) | async-done | bytes 2097184 | tf_op jit(solution)/shard_map/all_to_all | solution.py:56
  188.1 4.6 %gather_fusion.1 = bf16[512,1024]{1,0:T(8,128)(2,1)S(1)} fusion(bf16[1024,1024]{1,0:T(8,128)(2,1)} %bitcast.15, s32[1024]{0:T(1024)S(1)} %pad_clamp_fusion), kind=kCustom, calls=%fused_computation.1 | custom fusion | bytes 2099200 | tf_op jit(solution)/shard_map/gather | solution.py:59
  192.7 1.7 reshape.83
  194.4 0.0 copy-start.2
  194.4 3.0 %multiply_reduce_fusion = f32[128,1024]{1,0:T(8,128)S(1)} fusion(f32[128,4,1024]{2,1,0:T(4,128)} %reshape.83, f32[128,4]{1,0:T(8,128)S(1)} %copy.23), kind=kLoop, calls=%fused_computation.9 | loop fusion | flops 917504 | bytes 2623488 | tf_op jit(solution)/shard_map/reduce_sum | solution.py:60
  197.4 0.1 multiply_reduce_fusion.2
  197.5 2.5 %psum.7 = f32[128]{0:T(128)S(1)} all-reduce(f32[128]{0:T(128)S(1)} %multiply_reduce_fusion.2), channel_id=1, replica_groups=mesh['grp'=2,'ep'=8,'tp'=2] {'tp'}, use_global_device_ids=true, to_apply=%region_8.9 | all-reduce | flops 128 | bytes 1024 | tf_op jit(solution)/shard_map/psum | solution.py:62
  200.0 0.0 copy-done.2
  200.0 0.8 multiply_convert_fusion
  (12 shorter events, 0.1 us)
Async XLA Ops:
  6.5 103.2 %copy-start = (bf16[2,256,2048]{2,1,0:T(8,128)(2,1)S(1)}, bf16[2,256,2048]{2,1,0:T(8,128)(2,1)}, u32[]{:S(2)}) copy-start(bf16[2,256,2048]{2,1,0:T(8,128)(2,1)} %param.14) | copy-start | bytes 6291460
  6.5 2.5 %copy-start.1 = (s32[128,4]{0,1:T(4,128)S(1)}, s32[128,4]{0,1:T(4,128)}, u32[]{:S(2)}) copy-start(s32[128,4]{0,1:T(4,128)} %param.10) | copy-start | bytes 6148
  6.5 7.2 %copy-start.4 = (f32[2048]{0:T(1024)S(1)}, f32[2048]{0:T(1024)}, u32[]{:S(2)}) copy-start(f32[2048]{0:T(1024)} %param.9) | copy-start | bytes 24580
  6.5 82.8 %all-gather.3.cloned.1.call-start = ((), (), s32[]{:S(2)}) async-start(), calls=%async_computation.4 | async-start | bytes 6291456 | tf_op jit(solution)/shard_map/all_gather | solution.py:48
  76.5 53.8 %reduce-scatter.2.cloned.1.call-start = ((), (), s32[]{:S(2)}) async-start(), calls=%async_computation.3 | async-start | bytes 6291456 | tf_op jit(solution)/shard_map/reduce_scatter | solution.py:53
  133.4 6.0 %copy-start.3 = (f32[128,4]{0,1:T(4,128)S(1)}, f32[128,4]{0,1:T(4,128)}, u32[]{:S(2)}) copy-start(f32[128,4]{0,1:T(4,128)} %param.11) | copy-start | bytes 6148
  133.4 54.7 %all-to-all-start.1 = ((bf16[8,2,64,1024]{3,2,1,0:T(8,128)(2,1)}), bf16[8,2,64,1024]{3,2,1,0:T(8,128)(2,1)}, u32[]{:S(2)}, u32[]{:S(2)}) async-start(bf16[8,2,64,1024]{3,2,1,0:T(8,128)(2,1)} %copy.22), calls=%async_computation.2 | async-start | bytes 4194304 | tf_op jit(solution)/shard_map/all_to_all | solution.py:56
  194.4 5.6 %copy-start.2 = (f32[1024]{0:T(1024)S(1)}, f32[1024]{0:T(1024)}, u32[]{:S(2)}) copy-start(f32[1024]{0:T(1024)} %param.15) | copy-start | bytes 12292
Sparse Core Ops, SparseCore 0:
  76.6 12.6 all-gather.2
  117.2 13.0 reduce-scatter.1
